TPU v7x, 128 devices: a whole 4x4x4 slice. The times are simulated.
128 devices in a mesh: sp: 16 (over z, x), dp: 8 (over y, core).
Axes of the slice: x: 4, y: 4, z: 4, core: 2. Of those that a mesh axis runs over, the one named last changes fastest.
Arguments:
- queries: bfloat16 [8, 2048, 16, 128], P('dp', 'sp'), may hold values from -6 to 6
- key_rows: bfloat16 [8, 2048, 4, 128], P('dp', 'sp'), may hold values from -6 to 6
- values: bfloat16 [8, 2048, 4, 128], P('dp', 'sp'), may hold values from -6 to 6
- query_gain: float32 [128], replicated, may hold values from 0.4 to 5
- key_gain: float32 [128], replicated, may hold values from 0.4 to 5
- out_weight: bfloat16 [2048, 2048], P('sp', 'dp'), may hold values from -0.125 to 0.125
- residual: bfloat16 [8, 2048, 2048], P('dp', 'sp'), may hold values from -6 to 6
- norm_gain: float32 [2048], replicated, may hold values from 0.1 to 1.9
- expert_gate: bfloat16 [16, 2048, 1792], P('sp'), may hold values from -0.125 to 0.125
- expert_up: bfloat16 [16, 2048, 1792], P('sp'), may hold values from -0.125 to 0.125
- expert_down: bfloat16 [16, 1792, 2048], P('sp'), may hold values from -0.125 to 0.125
- routes: int32 [8, 2048, 2], P('dp', 'sp'), may hold values from 0 to 15, all different within a row; in each aligned block of 64 rows (0 to 63, 64 to 127, ..., all dimensions but the last counted through in order) at most 16 rows name the same one
- route_weight: float32 [8, 2048, 2], P('dp', 'sp'), may hold values from 0.25 to 1
Outputs:
- layer_out: bfloat16 [8, 2048, 2048], P('dp', 'sp')
Inputs may be any that keep to these rules, and one draw needn't show every extreme that they name: `routes`: in each aligned block of 64 rows of one device, no expert is named by more than 16 entries, a bound that some block reaches; the two experts of a row differ.
All inputs are finite; a program needn't handle non-finite values.
Results may differ from a plain program's by a relative error of at most 0.0095.
The roundings to bfloat16 on the way count: a program that leaves them out, or rounds other values in their place, can miss the bound.
Values may be sent and summed in bfloat16 or wider, within the bound.
A program may use at most 128 MiB of HBM per device.

v0:
```python
import jax
import jax.numpy as jnp
from jax import lax
from jax.sharding import PartitionSpec as P

GRID_W = 64


EPS = 1e-06
THETA = 10000.0


def rotate_half(vector, position):
    half_size = vector.shape[-1] // 2
    inverse = THETA ** (-jnp.arange(half_size, dtype=jnp.float32) / half_size)
    angles = position[:, None] * inverse[None, :]
    cosine = jnp.cos(angles)[:, None, :]
    sine_part = jnp.sin(angles)[:, None, :]
    first_part = vector[..., :half_size]
    second_part = vector[..., half_size:]
    return jnp.concatenate(
        [
            first_part * cosine - second_part * sine_part,
            first_part * sine_part + second_part * cosine,
        ],
        axis=-1,
    )


def normalize_rotate(vector, gain, positions):
    as_float = vector.astype(jnp.float32)
    scaled = (
        as_float * lax.rsqrt(jnp.mean(as_float * as_float, axis=-1, keepdims=True) + EPS) * gain
    )
    grid_row = (positions // GRID_W).astype(jnp.float32)
    column = (positions % GRID_W).astype(jnp.float32)
    quarter = scaled.shape[-1] // 2
    turned = jnp.concatenate(
        [rotate_half(scaled[..., :quarter], grid_row), rotate_half(scaled[..., quarter:], column)],
        axis=-1,
    )
    return turned.astype(jnp.bfloat16)


def softmax_rows(scores):
    row_max = jnp.max(scores, axis=-1, keepdims=True)
    exponent = jnp.exp(scores - row_max)
    return (exponent / jnp.sum(exponent, axis=-1, keepdims=True)).astype(jnp.bfloat16)


def attend_block(query_rows, key_rows, value_rows):
    scores = jnp.einsum(
        "qd,kd->qk", query_rows, key_rows, preferred_element_type=jnp.float32
    ) * query_rows.shape[-1] ** (-0.5)
    weights = softmax_rows(scores)
    return jnp.dot(weights, value_rows, preferred_element_type=jnp.float32).astype(jnp.bfloat16)


def attend_heads(head_query, head_key, head_value):
    length, head_count, head_width = head_query.shape
    block_size = min(512, length)
    key_slice = head_key[:, 0]
    value_slice = head_value[:, 0]
    query_blocks = head_query[:, 0].reshape(length // block_size, block_size, head_width)

    def one_block(query_block):
        return attend_block(query_block, key_slice, value_slice)

    outputs = [lax.map(one_block, query_blocks).reshape(length, head_width)]
    return jnp.stack(outputs, axis=1)


def gather_columns(out_weight):
    return lax.all_gather(out_weight, "dp", axis=1, tiled=True)


def project_tokens(attended, out_weight):
    out_cols = gather_columns(out_weight)
    return jnp.dot(
        attended,
        lax.all_gather(out_cols, "sp", axis=0, tiled=True),
        preferred_element_type=jnp.float32,
    )


def on_device(
    queries,
    key_rows,
    values,
    query_gain,
    key_gain,
    out_weight,
    residual,
    norm_gain,
    expert_gate,
    expert_up,
    expert_down,
    routes,
    route_weight,
):
    tok_count = queries.shape[1]
    head_count = queries.shape[2]
    head_width = queries.shape[3]
    group_size = head_count // key_rows.shape[2]
    positions = lax.axis_index("sp") * tok_count + jnp.arange(tok_count, dtype=jnp.int32)
    rot_query = normalize_rotate(queries[0], query_gain, positions)
    rot_key = normalize_rotate(key_rows[0], key_gain, positions)
    value_rows = values[0]
    head_query, head_key, head_value = (
        lax.all_to_all(rot_query, "sp", split_axis=1, concat_axis=0, tiled=True),
        lax.all_to_all(
            jnp.repeat(rot_key, group_size, axis=1), "sp", split_axis=1, concat_axis=0, tiled=True
        ),
        lax.all_to_all(
            jnp.repeat(value_rows, group_size, axis=1),
            "sp",
            split_axis=1,
            concat_axis=0,
            tiled=True,
        ),
    )
    by_heads = attend_heads(head_query, head_key, head_value)
    returned_heads = lax.all_to_all(by_heads, "sp", split_axis=0, concat_axis=1, tiled=True)
    projected = project_tokens(
        returned_heads.reshape(tok_count, head_count * head_width), out_weight
    )
    mixed_sum = residual[0].astype(jnp.float32) + projected
    normed = (
        mixed_sum
        * lax.rsqrt(jnp.mean(mixed_sum * mixed_sum, axis=-1, keepdims=True) + EPS)
        * norm_gain
    ).astype(jnp.bfloat16)
    experts = expert_gate.shape[0] * lax.axis_size("sp")
    half_rows = tok_count // 2
    capacity = max(2, 4 * half_rows // experts)
    chosen = routes[0].reshape(2, half_rows * 2)
    onehot = (chosen[..., None] == jnp.arange(experts, dtype=jnp.int32)).astype(jnp.int32)
    slot_rank = jnp.sum(jnp.cumsum(onehot, axis=1) * onehot, axis=-1) - 1
    slot_index = jnp.arange(2, dtype=jnp.int32)[:, None] * capacity + slot_rank
    target = (chosen * (2 * capacity) + slot_index).reshape(-1)
    model_width = normed.shape[1]
    filled = (
        jnp.zeros((experts * 2 * capacity, model_width), jnp.bfloat16)
        .at[target]
        .set(jnp.repeat(normed, 2, axis=0))
    )
    buffer = filled.reshape(experts, 2 * capacity, model_width)
    slot_batch = lax.all_to_all(buffer, "sp", split_axis=0, concat_axis=0, tiled=True)
    sources, slot_count, feature_count = slot_batch.shape
    flat_rows = slot_batch.reshape(sources * slot_count, feature_count)
    gate_part = jnp.dot(flat_rows, expert_gate[0], preferred_element_type=jnp.float32)
    up_part = jnp.dot(flat_rows, expert_up[0], preferred_element_type=jnp.float32)
    hidden = (jax.nn.silu(gate_part) * up_part).astype(jnp.bfloat16)
    expert_result = jnp.dot(hidden, expert_down[0], preferred_element_type=jnp.float32).astype(
        jnp.bfloat16
    )
    served = expert_result.reshape(sources, slot_count, feature_count)
    returned = lax.all_to_all(served, "sp", split_axis=0, concat_axis=0, tiled=True)
    picked = (
        returned.reshape(-1, model_width)[target]
        .astype(jnp.float32)
        .reshape(tok_count, 2, model_width)
    )
    result = mixed_sum + jnp.sum(picked * route_weight[0][..., None], axis=1)
    return result.astype(jnp.bfloat16)[None]


def solution(mesh):
    in_specs = (
        P("dp", "sp", None, None),
        P("dp", "sp", None, None),
        P("dp", "sp", None, None),
        P(),
        P(),
        P("sp", "dp"),
        P("dp", "sp", None),
        P(),
        P("sp", None, None),
        P("sp", None, None),
        P("sp", None, None),
        P("dp", "sp", None),
        P("dp", "sp", None),
    )
    out_specs = P("dp", "sp", None)
    return jax.shard_map(
        on_device, mesh=mesh, in_specs=in_specs, out_specs=out_specs, check_vma=False
    )
```

profile of v0, /device:TPU:8, one launch (start us, length us, event | category | flops | bytes accessed | tf_op | source)
XLA Modules:
  0.0 227.7 jit_solution(17843806459797019418)
XLA Ops:
  6.5 14.7 %all_gather.6 = bf16[128,2048]{1,0:T(8,128)(2,1)} all-gather(bf16[128,256]{1,0:T(8,128)(2,1)} %param.20), channel_id=1, replica_groups=mesh['sp'=16,'dp'=8] {'dp'}, dimensions={1}, use_global_device_ids=true | all-gather | bytes 589824 | tf_op jit(solution)/shard_map/all_gather | solution.py:74
  21.3 1.1 fusion.28
  22.5 0.5 multiply_cosine_fusion.1
  23.0 1.1 fusion.29
  24.1 0.5 subtract_convert_fusion.3
  24.6 0.4 pad_maximum_fusion.1
  25.1 1.0 broadcast_in_dim.16
  26.1 7.9 %all-to-all-start.1 = ((bf16[128,16,128]{2,0,1:T(8,128)(2,1)}), bf16[128,16,128]{2,0,1:T(8,128)(2,1)S(1)}, u32[]{:S(2)}, u32[]{:S(2)}) async-start(bf16[128,16,128]{2,0,1:T(8,128)(2,1)} %bitcast.10), calls=%async_computation.1 | async-start | bytes 1048576 | tf_op jit(solution)/shard_map/all_to_all | solution.py:111
  33.9 0.3 fusion.23
  34.3 0.3 fusion.24
  34.7 0.9 subtract_convert_fusion.1
  35.6 1.5 pad_maximum_fusion
  37.0 14.5 %all-to-all-done.1 = bf16[128,16,128]{2,0,1:T(8,128)(2,1)S(1)} async-done(((bf16[128,16,128]{2,0,1:T(8,128)(2,1)}), bf16[128,16,128]{2,0,1:T(8,128)(2,1)S(1)}, u32[]{:S(2)}, u32[]{:S(2)}) %all-to-all-start.1) | async-done | bytes 524320 | tf_op jit(solution)/shard_map/all_to_all | solution.py:111
  51.6 3.6 %all-to-all-start = ((bf16[128,16,128]{2,0,1:T(8,128)(2,1)}), bf16[128,16,128]{2,0,1:T(8,128)(2,1)S(1)}, u32[]{:S(2)}, u32[]{:S(2)}) async-start(bf16[128,16,128]{2,0,1:T(8,128)(2,1)} %pad_maximum_fusion), calls=%async_computation | async-start | bytes 1048576 | tf_op jit(solution)/shard_map/all_to_all | solution.py:110
  55.2 0.1 copy.63
  55.3 0.1 eq.18
  55.4 10.9 %all-to-all-done = bf16[128,16,128]{2,0,1:T(8,128)(2,1)S(1)} async-done(((bf16[128,16,128]{2,0,1:T(8,128)(2,1)}), bf16[128,16,128]{2,0,1:T(8,128)(2,1)S(1)}, u32[]{:S(2)}, u32[]{:S(2)}) %all-to-all-start) | async-done | bytes 524320 | tf_op jit(solution)/shard_map/all_to_all | solution.py:110
  66.3 0.9 broadcast_in_dim.17
  67.2 3.6 %all-to-all-start.2 = ((bf16[128,16,128]{2,0,1:T(8,128)(2,1)}), bf16[128,16,128]{2,0,1:T(8,128)(2,1)S(1)}, u32[]{:S(2)}, u32[]{:S(2)}) async-start(bf16[128,16,128]{2,0,1:T(8,128)(2,1)} %bitcast.15), calls=%async_computation.2 | async-start | bytes 1048576 | tf_op jit(solution)/shard_map/all_to_all | solution.py:114
  70.8 0.1 fusion.30
  70.9 0.2 reduce_window_sum.11
  71.1 0.2 select_reduce_fusion
  71.3 17.2 %all-to-all-done.2 = bf16[128,16,128]{2,0,1:T(8,128)(2,1)S(1)} async-done(((bf16[128,16,128]{2,0,1:T(8,128)(2,1)}), bf16[128,16,128]{2,0,1:T(8,128)(2,1)S(1)}, u32[]{:S(2)}, u32[]{:S(2)}) %all-to-all-start.2) | async-done | bytes 524320 | tf_op jit(solution)/shard_map/all_to_all | solution.py:114
  88.5 10.7 %while.10 = (s32[]{:T(128)}, bf16[4,512,128]{2,1,0:T(8,128)(2,1)S(1)}, bf16[4,512,128]{2,1,0:T(8,128)(2,1)S(1)}, bf16[2048,128]{1,0:T(8,128)(2,1)S(1)}, bf16[2048,128]{1,0:T(8,128)(2,1)S(1)}, /*index=5*/s32[]{:T(128)}) while((s32[]{:T(128)}, bf16[4,512,128]{2,1,0:T(8,128)(2,1)S(1)}, bf16[4,512,128]{2,1,0:T(8,128)(2,1)S(1)}, ...), condition=%wide.region_5.6_spmd, body=%wide.region_2.5_spmd.sunk | while | flops 546372608 | bytes 13903949 | solution.py:69
  88.5 0.8 multiply_reduce_fusion.4
  89.3 0.8 fusion.46
  90.1 1.1 fusion.47
  91.2 0.8 multiply_reduce_fusion.4
  91.9 0.8 fusion.46
  92.8 1.1 fusion.47
  93.8 0.8 multiply_reduce_fusion.4
  94.6 0.8 fusion.46
  95.4 1.1 fusion.47
  96.5 0.8 multiply_reduce_fusion.4
  97.3 0.8 fusion.46
  98.1 1.1 fusion.47
  99.2 0.5 broadcast.285
  99.7 1.1 reduce
  100.8 0.9 reshape.289
  101.7 3.8 %all-to-all-start.3 = ((bf16[16,2,8192]{2,1,0:T(2,128)(2,1)}), bf16[16,2,8192]{2,1,0:T(2,128)(2,1)S(1)}, u32[]{:S(2)}, u32[]{:S(2)}) async-start(bf16[16,2,8192]{2,1,0:T(2,128)(2,1)} %reshape.289), calls=%async_computation.3 | async-start | bytes 1048576 | tf_op jit(solution)/shard_map/all_to_all | solution.py:123
  105.5 0.1 copy.62
  105.6 0.1 mul.316
  105.7 0.1 add_add_fusion
  105.8 9.6 %all-to-all-done.3 = bf16[16,2,8192]{2,1,0:T(2,128)(2,1)S(1)} async-done(((bf16[16,2,8192]{2,1,0:T(2,128)(2,1)}), bf16[16,2,8192]{2,1,0:T(2,128)(2,1)S(1)}, u32[]{:S(2)}, u32[]{:S(2)}) %all-to-all-start.3) | async-done | bytes 524320 | tf_op jit(solution)/shard_map/all_to_all | solution.py:123
  115.4 0.5 reshape.290
  115.9 0.1 copy.65
  116.0 0.3 copy.61
  116.3 0.0 all-gather.2.cloned.1.call-done
  116.3 4.7 %multiply_reduce_fusion.2 = (f32[128]{0:T(128)S(1)}, f32[128,2048]{1,0:T(8,128)S(1)}) fusion(bf16[128,2048]{0,1:T(8,128)(2,1)S(1)} %bitcast.84, bf16[2048,2048]{1,0:T(8,128)(2,1)} %all-gather.2.cloned.1.call-done, bf16[1,128,2048]{2,1,0:T(8,128)(2,1)S(1)} %copy-done.2), kind=kOutput, calls=%fused_computation.31 | convolution fusion | flops 1074790272 | bytes 10486272 | tf_op jit(solution)/shard_map/dot_general | solution.py:79
  121.1 0.2 multiply_convert_fusion.1
  121.2 0.6 broadcast_in_dim.19
  121.9 1.2 reshape.283
  123.1 3.5 %scatter_custom_fusion = bf16[512,2048]{1,0:T(8,128)(2,1)S(1)} fusion(s32[256]{0:T(256)S(1)} %bitcast.93, bf16[256,2048]{1,0:T(8,128)(2,1)} %reshape.283, bf16[]{:T(256)} %constant.76.clone.1), kind=kCustom, calls=%fused_computation.32 | custom fusion | bytes 2097664 | tf_op jit(solution)/shard_map/scatter | solution.py:145
  126.6 27.9 %all_to_all.70 = bf16[16,32,2048]{2,1,0:T(8,128)(2,1)S(1)} all-to-all(bf16[16,32,2048]{2,1,0:T(8,128)(2,1)S(1)} %bitcast.83), channel_id=1, replica_groups=mesh['sp'=16,'dp'=8] {'sp'}, dimensions={0} | all-to-all | bytes 4194304 | tf_op jit(solution)/shard_map/all_to_all | solution.py:148
  154.5 1.3 copy-done
  155.9 8.8 %fusion.14 = f32[512,1792]{1,0:T(8,128)} fusion(bf16[512,2048]{1,0:T(8,128)(2,1)S(1)} %bitcast.88, bf16[1,2048,1792]{2,1,0:T(8,128)(2,1)} %param.23), kind=kOutput, calls=%fused_computation.19 | convolution fusion | flops 3758096384 | bytes 13107200 | tf_op jit(solution)/shard_map/dot_general | solution.py:151
  164.7 16.9 %fusion.18 = bf16[512,2048]{1,0:T(8,128)(2,1)} fusion(bf16[1,1792,2048]{2,1,0:T(8,128)(2,1)} %param.25, f32[512,1792]{1,0:T(8,128)} %fusion.14, bf16[512,2048]{1,0:T(8,128)(2,1)} %bitcast.89, bf16[1,2048,1792]{2,1,0:T(8,128)(2,1)} %param.24), kind=kOutput, calls=%fused_computation.22 | convolution fusion | flops 7522746368 | bytes 22544384 | tf_op jit(solution)/shard_map/dot_general | solution.py:154
  181.7 4.1 %all-to-all-start.5 = ((bf16[16,32,2048]{2,1,0:T(8,128)(2,1)}), bf16[16,32,2048]{2,1,0:T(8,128)(2,1)S(1)}, u32[]{:S(2)}, u32[]{:S(2)}) async-start(bf16[16,32,2048]{2,1,0:T(8,128)(2,1)} %bitcast.87), calls=%async_computation.5 | async-start | bytes 4194304 | tf_op jit(solution)/shard_map/all_to_all | solution.py:158
  185.8 0.1 copy.64
  185.9 26.1 %all-to-all-done.5 = bf16[16,32,2048]{2,1,0:T(8,128)(2,1)S(1)} async-done(((bf16[16,32,2048]{2,1,0:T(8,128)(2,1)}), bf16[16,32,2048]{2,1,0:T(8,128)(2,1)S(1)}, u32[]{:S(2)}, u32[]{:S(2)}) %all-to-all-start.5) | async-done | bytes 2097184 | tf_op jit(solution)/shard_map/all_to_all | solution.py:158
  212.0 2.3 %gather_fusion = bf16[256,2048]{1,0:T(8,128)(2,1)} fusion(bf16[512,2048]{1,0:T(8,128)(2,1)S(1)} %bitcast.81, s32[1024]{0:T(1024)S(1)} %pad_clamp_fusion), kind=kCustom, calls=%fused_computation | custom fusion | bytes 2098176 | tf_op jit(solution)/shard_map/gather | solution.py:160
  214.4 2.4 %reshape.270 = f32[128,2,2048]{2,1,0:T(2,128)S(1)} reshape(bf16[256,2048]{1,0:T(8,128)(2,1)} %gather_fusion) | data formatting | bytes 3145728 | tf_op jit(solution)/shard_map/convert_element_type | solution.py:161
  216.8 3.2 %multiply_reduce_fusion.1 = f32[128,2048]{1,0:T(8,128)S(1)} fusion(f32[128,2,2048]{2,1,0:T(2,128)S(1)} %reshape.270, f32[128,2]{1,0:T(8,128)S(1)} %copy.64), kind=kLoop, calls=%fused_computation.24 | loop fusion | flops 786432 | bytes 3146752 | tf_op jit(solution)/shard_map/reduce_sum | solution.py:164
  219.9 0.9 fusion.27
  (29 shorter events, 0.2 us)
Async XLA Ops:
  6.5 27.4 %copy-start.1 = (bf16[1,128,16,128]{3,2,1,0:T(8,128)(2,1)S(1)}, bf16[1,128,16,128]{3,2,1,0:T(8,128)(2,1)}, u32[]{:S(2)}) copy-start(bf16[1,128,16,128]{3,2,1,0:T(8,128)(2,1)} %param.15) | copy-start | bytes 1572868
  6.5 27.8 %copy-start.7 = (f32[128]{0:T(128)S(1)}, f32[128]{0:T(128)}, u32[]{:S(2)}) copy-start(f32[128]{0:T(128)} %param.18) | copy-start | bytes 1540
  6.5 109.7 %all-gather.2.cloned.1.call-start = ((), (), s32[]{:S(2)}) async-start(), calls=%async_computation.6 | async-start | bytes 8912896 | tf_op jit(solution)/shard_map/all_gather | solution.py:81
  26.1 25.5 %all-to-all-start.1 = ((bf16[128,16,128]{2,0,1:T(8,128)(2,1)}), bf16[128,16,128]{2,0,1:T(8,128)(2,1)S(1)}, u32[]{:S(2)}, u32[]{:S(2)}) async-start(bf16[128,16,128]{2,0,1:T(8,128)(2,1)} %bitcast.10), calls=%async_computation.1 | async-start | bytes 1048576 | tf_op jit(solution)/shard_map/all_to_all | solution.py:111
  34.7 20.5 %copy-start.3 = (bf16[1,128,4,128]{3,2,1,0:T(4,128)(2,1)S(1)}, bf16[1,128,4,128]{3,2,1,0:T(4,128)(2,1)}, u32[]{:S(2)}) copy-start(bf16[1,128,4,128]{3,2,1,0:T(4,128)(2,1)} %param.17) | copy-start | bytes 393220
  34.7 20.5 %copy-start.5 = (s32[1,128,2]{1,2,0:T(2,128)S(1)}, s32[1,128,2]{1,2,0:T(2,128)}, u32[]{:S(2)}) copy-start(s32[1,128,2]{1,2,0:T(2,128)} %param.26) | copy-start | bytes 3076
  51.6 14.8 %all-to-all-start = ((bf16[128,16,128]{2,0,1:T(8,128)(2,1)}), bf16[128,16,128]{2,0,1:T(8,128)(2,1)S(1)}, u32[]{:S(2)}, u32[]{:S(2)}) async-start(bf16[128,16,128]{2,0,1:T(8,128)(2,1)} %pad_maximum_fusion), calls=%async_computation | async-start | bytes 1048576 | tf_op jit(solution)/shard_map/all_to_all | solution.py:110
  67.2 21.3 %all-to-all-start.2 = ((bf16[128,16,128]{2,0,1:T(8,128)(2,1)}), bf16[128,16,128]{2,0,1:T(8,128)(2,1)S(1)}, u32[]{:S(2)}, u32[]{:S(2)}) async-start(bf16[128,16,128]{2,0,1:T(8,128)(2,1)} %bitcast.15), calls=%async_computation.2 | async-start | bytes 1048576 | tf_op jit(solution)/shard_map/all_to_all | solution.py:114
  99.7 16.6 %copy-start.2 = (bf16[1,128,2048]{2,1,0:T(8,128)(2,1)S(1)}, bf16[1,128,2048]{2,1,0:T(8,128)(2,1)}, u32[]{:S(2)}) copy-start(bf16[1,128,2048]{2,1,0:T(8,128)(2,1)} %param.21) | copy-start | bytes 1572868
  101.7 13.7 %all-to-all-start.3 = ((bf16[16,2,8192]{2,1,0:T(2,128)(2,1)}), bf16[16,2,8192]{2,1,0:T(2,128)(2,1)S(1)}, u32[]{:S(2)}, u32[]{:S(2)}) async-start(bf16[16,2,8192]{2,1,0:T(2,128)(2,1)} %reshape.289), calls=%async_computation.3 | async-start | bytes 1048576 | tf_op jit(solution)/shard_map/all_to_all | solution.py:123
  116.3 4.8 %copy-start.4 = (f32[2048]{0:T(1024)S(1)}, f32[2048]{0:T(1024)}, u32[]{:S(2)}) copy-start(f32[2048]{0:T(1024)} %param.22) | copy-start | bytes 24580
  154.5 1.3 copy-start
  181.7 4.1 %copy-start.6 = (f32[1,128,2]{1,2,0:T(2,128)S(1)}, f32[1,128,2]{1,2,0:T(2,128)}, u32[]{:S(2)}) copy-start(f32[1,128,2]{1,2,0:T(2,128)} %param.27) | copy-start | bytes 3076
  181.7 30.3 %all-to-all-start.5 = ((bf16[16,32,2048]{2,1,0:T(8,128)(2,1)}), bf16[16,32,2048]{2,1,0:T(8,128)(2,1)S(1)}, u32[]{:S(2)}, u32[]{:S(2)}) async-start(bf16[16,32,2048]{2,1,0:T(8,128)(2,1)} %bitcast.87), calls=%async_computation.5 | async-start | bytes 4194304 | tf_op jit(solution)/shard_map/all_to_all | solution.py:158
Sparse Core Ops, SparseCore 0:
  21.4 83.8 all-gather.1
where the time goes:
time: 229 us; the launch traced here: 228 us
  waiting for transfers between devices  78.3 us (34%)
  blocking collectives  42.7 us (19%)
  matrix products  37.9 us (17%)
  starting transfers between devices  22.9 us (10%)
  local copies, waits for them, and re-layouts  16.3 us (7%)
  other arithmetic  15.9 us (7%)
  between operations  13.7 us (6%)
    all_to_all x1, blocking collectives, on_device(): lax.all_to_all(buffer, 'sp', split_axis=0, concat_axis=0, tiled=True)  27.9 us
    all_to_all x1, waiting for transfers between devices, on_device(): lax.all_to_all(served, 'sp', split_axis=0, concat_axis=0, tiled=True)  26.1 us
    all_to_all x1, waiting for transfers between devices, on_device(): lax.all_to_all(jnp.repeat(value_rows, group_size, axis=1), 'sp', split_ax...  17.2 us
    dot_general x1, matrix products, on_device(): jnp.dot(hidden, expert_down[0], preferred_element_type=jnp.float32)  16.9 us
    all_gather x1, blocking collectives, gather_columns(): return lax.all_gather(out_weight, 'dp', axis=1, tiled=True)  14.7 us
    all_to_all x1, waiting for transfers between devices, on_device(): lax.all_to_all(jnp.repeat(rot_key, group_size, axis=1), 'sp', split_axis=...  14.5 us
    all_to_all x1, waiting for transfers between devices, on_device(): lax.all_to_all(rot_query, 'sp', split_axis=1, concat_axis=0, tiled=True)  10.9 us
    all_to_all x1, waiting for transfers between devices, on_device(): lax.all_to_all(by_heads, 'sp', split_axis=0, concat_axis=1, tiled=True)  9.58 us
  transfers between devices with their start and end apart: 6, of which 5 were waited for; matrix products, arithmetic and copies ran while one was open for 10% of the time, Pallas kernels for 0%

commit v1 on v0

--- a/solution.py
+++ b/solution.py
@@ -1,7 +1,11 @@
 import jax
 import jax.numpy as jnp
 from jax import lax
+from jax.experimental import pallas as pl
+from jax.experimental.pallas import tpu as pltpu
 from jax.sharding import PartitionSpec as P
+
+MESH = pl.DeviceIdType.MESH
 
 GRID_W = 64
 
@@ -125,44 +129,175 @@
         returned_heads.reshape(tok_count, head_count * head_width), out_weight
     )
     mixed_sum = residual[0].astype(jnp.float32) + projected
-    normed = (
-        mixed_sum
-        * lax.rsqrt(jnp.mean(mixed_sum * mixed_sum, axis=-1, keepdims=True) + EPS)
-        * norm_gain
-    ).astype(jnp.bfloat16)
-    experts = expert_gate.shape[0] * lax.axis_size("sp")
-    half_rows = tok_count // 2
-    capacity = max(2, 4 * half_rows // experts)
-    chosen = routes[0].reshape(2, half_rows * 2)
-    onehot = (chosen[..., None] == jnp.arange(experts, dtype=jnp.int32)).astype(jnp.int32)
-    slot_rank = jnp.sum(jnp.cumsum(onehot, axis=1) * onehot, axis=-1) - 1
-    slot_index = jnp.arange(2, dtype=jnp.int32)[:, None] * capacity + slot_rank
-    target = (chosen * (2 * capacity) + slot_index).reshape(-1)
-    model_width = normed.shape[1]
-    filled = (
-        jnp.zeros((experts * 2 * capacity, model_width), jnp.bfloat16)
-        .at[target]
-        .set(jnp.repeat(normed, 2, axis=0))
-    )
-    buffer = filled.reshape(experts, 2 * capacity, model_width)
-    slot_batch = lax.all_to_all(buffer, "sp", split_axis=0, concat_axis=0, tiled=True)
-    sources, slot_count, feature_count = slot_batch.shape
-    flat_rows = slot_batch.reshape(sources * slot_count, feature_count)
-    gate_part = jnp.dot(flat_rows, expert_gate[0], preferred_element_type=jnp.float32)
-    up_part = jnp.dot(flat_rows, expert_up[0], preferred_element_type=jnp.float32)
-    hidden = (jax.nn.silu(gate_part) * up_part).astype(jnp.bfloat16)
-    expert_result = jnp.dot(hidden, expert_down[0], preferred_element_type=jnp.float32).astype(
-        jnp.bfloat16
-    )
-    served = expert_result.reshape(sources, slot_count, feature_count)
-    returned = lax.all_to_all(served, "sp", split_axis=0, concat_axis=0, tiled=True)
-    picked = (
-        returned.reshape(-1, model_width)[target]
-        .astype(jnp.float32)
-        .reshape(tok_count, 2, model_width)
-    )
-    result = mixed_sum + jnp.sum(picked * route_weight[0][..., None], axis=1)
-    return result.astype(jnp.bfloat16)[None]
+    return moe(
+        mixed_sum, norm_gain, routes[0], route_weight[0], expert_gate[0], expert_up[0], expert_down[0]
+    )[None]
+
+
+def offset_of(i):
+    q = i // 4
+    return (q % 2) * 2 + q // 2, i % 4
+
+
+def peer_of(z, x, dz, dx):
+    return ((z + dz) % 4) * 4 + (x + dx) % 4
+
+
+def experts_of_slots(slots, z, x):
+    i = slots >> 5
+    q = i >> 2
+    dz = ((q & 1) << 1) | (q >> 1)
+    return (((z + dz) & 3) << 2) | ((x + (i & 3)) & 3)
+
+
+def to_bf16(mask):
+    return jnp.where(mask, 1.0, 0.0).astype(jnp.bfloat16)
+
+
+def moe_kernel(
+    mixed_ref, gain_ref, routes_ref, routes_t_ref, weight_ref, gate_hbm, up_hbm, down_hbm,
+    out_ref,
+    gate_v, up_v, down_v, send_v, recv_v, res_v, ret_v, hid_v,
+    w_sem, ds_sem, dr_sem, rs_sem, rr_sem,
+):
+    me = lax.axis_index("sp")
+    z, x = me // 4, me % 4
+    loads = [
+        pltpu.make_async_copy(src, dst, w_sem.at[n])
+        for n, (src, dst) in enumerate(((gate_hbm, gate_v), (up_hbm, up_v), (down_hbm, down_v)))
+    ]
+    for load in loads:
+        load.start()
+    barrier = pltpu.get_barrier_semaphore()
+    for i in range(1, 16):
+        dz, dx = offset_of(i)
+        pl.semaphore_signal(
+            barrier, inc=1, device_id={"sp": peer_of(z, x, dz, dx)}, device_id_type=MESH
+        )
+
+    mixed = mixed_ref[...]
+    scale = lax.rsqrt(jnp.mean(mixed * mixed, axis=-1, keepdims=True) + EPS)
+    normed = (mixed * scale * gain_ref[...]).astype(jnp.bfloat16)
+
+    slots = lax.broadcasted_iota(jnp.int32, (512, 128), 0)
+    rows = lax.broadcasted_iota(jnp.int32, (512, 128), 1)
+    expert = experts_of_slots(slots, z, x)
+    named = (routes_t_ref[0:1, :] == expert) | (routes_t_ref[1:2, :] == expert)
+    before_r = lax.broadcasted_iota(jnp.int32, (128, 128), 0)
+    before_c = lax.broadcasted_iota(jnp.int32, (128, 128), 1)
+    same = (before_r >> 6) == (before_c >> 6)
+    upper = to_bf16((before_r < before_c) & same)
+    lower = to_bf16((before_c < before_r) & same)
+    rank = jnp.dot(to_bf16(named), upper, preferred_element_type=jnp.float32)
+    wanted = ((slots & 31) - ((rows >> 6) << 4)).astype(jnp.float32)
+    pick = to_bf16(named & (rank == wanted))
+    for c in range(2):
+        part = slice(c * 256, c * 256 + 256)
+        for n in range(4):
+            cols = slice(n * 512, n * 512 + 512)
+            sent = jnp.dot(
+                pick[part], normed[:, cols], preferred_element_type=jnp.float32
+            ).astype(jnp.bfloat16)
+            send_v[part, cols] = sent
+            if c == 0:
+                recv_v[0:32, cols] = sent[0:32]
+    pl.semaphore_wait(barrier, 15)
+
+    def copy(i, src, dst, ssem, rsem, dz, dx):
+        return pltpu.make_async_remote_copy(
+            src_ref=src.at[pl.ds(i * 32, 32)],
+            dst_ref=dst.at[pl.ds(i * 32, 32)],
+            send_sem=ssem.at[i],
+            recv_sem=rsem.at[i],
+            device_id={"sp": peer_of(z, x, dz, dx)},
+            device_id_type=MESH,
+        )
+
+    outgoing = []
+    for i in range(1, 16):
+        dz, dx = offset_of(i)
+        outgoing.append(copy(i, send_v, recv_v, ds_sem, dr_sem, dz, dx))
+    for sending in outgoing:
+        sending.start()
+
+    slots_t = lax.broadcasted_iota(jnp.int32, (128, 512), 1)
+    rows_t = lax.broadcasted_iota(jnp.int32, (128, 512), 0)
+    expert_t = experts_of_slots(slots_t, z, x)
+    first = routes_ref[:, 0:1] == expert_t
+    second = routes_ref[:, 1:2] == expert_t
+    rank_t = jnp.dot(lower, to_bf16(first | second), preferred_element_type=jnp.float32)
+    here = rank_t == ((slots_t & 31) - ((rows_t >> 6) << 4)).astype(jnp.float32)
+    take_first = to_bf16(first & here)
+    take_second = to_bf16(second & here)
+
+    returning = []
+    for i in range(1, 16):
+        dz, dx = offset_of(i)
+        returning.append(copy(i, res_v, ret_v, rs_sem, rr_sem, -dz, -dx))
+    loads[0].wait()
+    loads[1].wait()
+    for c in range(2):
+        for i in range(max(1, c * 8), c * 8 + 8):
+            outgoing[i - 1].wait_recv()
+        part = slice(c * 256, c * 256 + 256)
+        for n in range(7):
+            cols = slice(n * 256, n * 256 + 256)
+            gate = jnp.dot(recv_v[part], gate_v[:, cols], preferred_element_type=jnp.float32)
+            up = jnp.dot(recv_v[part], up_v[:, cols], preferred_element_type=jnp.float32)
+            hid_v[:, cols] = (gate / (1.0 + jnp.exp(-gate)) * up).astype(jnp.bfloat16)
+        if c == 0:
+            loads[2].wait()
+        for n in range(8):
+            cols = slice(n * 256, n * 256 + 256)
+            done = jnp.dot(
+                hid_v[...], down_v[:, cols], preferred_element_type=jnp.float32
+            ).astype(jnp.bfloat16)
+            res_v[part, cols] = done
+            if c == 0:
+                ret_v[0:32, cols] = done[0:32]
+        for i in range(max(1, c * 8), c * 8 + 8):
+            returning[i - 1].start()
+    for back in returning:
+        back.wait_recv()
+    for n in range(4):
+        cols = slice(n * 512, n * 512 + 512)
+        got = ret_v[:, cols]
+        one = jnp.dot(take_first, got, preferred_element_type=jnp.float32)
+        two = jnp.dot(take_second, got, preferred_element_type=jnp.float32)
+        total = mixed_ref[:, cols] + (one * weight_ref[:, 0:1] + two * weight_ref[:, 1:2])
+        out_ref[:, cols] = total.astype(jnp.bfloat16)
+    for sending in outgoing:
+        sending.wait_send()
+    for back in returning:
+        back.wait_send()
+
+
+def moe(mixed_sum, norm_gain, routes, route_weight, gate, up, down):
+    vmem = pl.BlockSpec(memory_space=pltpu.VMEM)
+    hbm = pl.BlockSpec(memory_space=pl.ANY)
+    rows = pltpu.VMEM((512, 2048), jnp.bfloat16)
+    return pl.pallas_call(
+        moe_kernel,
+        out_shape=jax.ShapeDtypeStruct((128, 2048), jnp.bfloat16),
+        in_specs=[vmem] * 5 + [hbm] * 3,
+        out_specs=vmem,
+        scratch_shapes=[
+            pltpu.VMEM((2048, 1792), jnp.bfloat16),
+            pltpu.VMEM((2048, 1792), jnp.bfloat16),
+            pltpu.VMEM((1792, 2048), jnp.bfloat16),
+            rows, rows, rows, rows,
+            pltpu.VMEM((256, 1792), jnp.bfloat16),
+            pltpu.SemaphoreType.DMA((3,)),
+            pltpu.SemaphoreType.DMA((16,)),
+            pltpu.SemaphoreType.DMA((16,)),
+            pltpu.SemaphoreType.DMA((16,)),
+            pltpu.SemaphoreType.DMA((16,)),
+        ],
+        compiler_params=pltpu.CompilerParams(
+            collective_id=1, has_side_effects=True, vmem_limit_bytes=56 << 20
+        ),
+        name="experts",
+    )(mixed_sum, norm_gain.reshape(1, -1), routes, routes.T, route_weight, gate, up, down)
 
 
 def solution(mesh):

time: 229 us -> 188 us (0.82)
  Pallas kernels: 0 us -> 56.2 us
  blocking collectives: 42.7 us -> 14.7 us
  waiting for transfers between devices: 78.3 us -> 51.9 us
  matrix products: 37.9 us -> 13.1 us
  local copies, waits for them, and re-layouts: 16.3 us -> 7.74 us
  other arithmetic: 15.9 us -> 11.1 us
  starting transfers between devices: 22.9 us -> 18.6 us
    pallas_call x0 -> x1, Pallas kernels: none -> 56.2 us  [moe(): pl.pallas_call(moe_kernel, out_shape=jax.ShapeDtypeStruct((128, 2048), jn...]
    all_to_all x1 -> x0, blocking collectives: 27.9 us -> none  [on_device(): lax.all_to_all(buffer, 'sp', split_axis=0, concat_axis=0, tiled=True)]
    all_to_all x1 -> x0, waiting for transfers between devices: 26.1 us -> none  [on_device(): lax.all_to_all(served, 'sp', split_axis=0, concat_axis=0, tiled=True)]
    dot_general x2 -> x0, matrix products: 25.8 us -> none  [the longest x1 16.9 us: on_device(): jnp.dot(hidden, expert_down[0], preferred_element_type=jnp.float32)]
    all_to_all x1 -> x0, starting transfers between devices: 4.11 us -> none  [on_device(): lax.all_to_all(served, 'sp', split_axis=0, concat_axis=0, tiled=True)]
    scatter x1 -> x0, local copies, waits for them, and re-layouts: 3.5 us -> none  [on_device(): filled = jnp.zeros((experts * 2 * capacity, model_width), jnp.bfloat16).a...]
    reduce_sum x2 -> x0, other arithmetic: 3.34 us -> none  [the longest x1 3.16 us: on_device(): result = mixed_sum + jnp.sum(picked * route_weight[0][..., None], axis=1)]
    convert_element_type x1 -> x0, local copies, waits for them, and re-layouts: 2.37 us -> none  [on_device(): picked = returned.reshape(-1, model_width)[target].astype(jnp.float32).re...]
  transfers between devices with their start and end apart: 6 -> 5, of which waited for: 5 -> 4; matrix products, arithmetic and copies ran while one was open for 10% -> 13% of each run, Pallas kernels for 0% -> 0%
where the time goes in v1:
time: 188 us; the launch traced here: 187 us
  Pallas kernels  56.2 us (30%)
  waiting for transfers between devices  51.9 us (28%)
  starting transfers between devices  18.6 us (10%)
  blocking collectives  14.7 us (8%)
  between operations  13.6 us (7%)
  matrix products  13.1 us (7%)
  other arithmetic  11.1 us (6%)
  local copies, waits for them, and re-layouts  7.74 us (4%)
    pallas_call x1, Pallas kernels, moe(): pl.pallas_call(moe_kernel, out_shape=jax.ShapeDtypeStruct((128, 2048), jn...  56.2 us
    all_to_all x1, waiting for transfers between devices, on_device(): lax.all_to_all(jnp.repeat(value_rows, group_size, axis=1), 'sp', split_ax...  17.7 us
    all_gather x1, blocking collectives, gather_columns(): return lax.all_gather(out_weight, 'dp', axis=1, tiled=True)  14.7 us
    all_to_all x1, waiting for transfers between devices, on_device(): lax.all_to_all(jnp.repeat(rot_key, group_size, axis=1), 'sp', split_axis=...  14.5 us
    all_to_all x1, waiting for transfers between devices, on_device(): lax.all_to_all(rot_query, 'sp', split_axis=1, concat_axis=0, tiled=True)  11.1 us
    all_to_all x1, waiting for transfers between devices, on_device(): lax.all_to_all(by_heads, 'sp', split_axis=0, concat_axis=1, tiled=True)  8.62 us
    all_to_all x1, starting transfers between devices, on_device(): lax.all_to_all(jnp.repeat(rot_key, group_size, axis=1), 'sp', split_axis=...  7.88 us
    dot_general x1, matrix products, project_tokens(): jnp.dot(attended, lax.all_gather(out_cols, 'sp', axis=0, tiled=True), pre...  5.73 us
  transfers between devices with their start and end apart: 5, of which 4 were waited for; matrix products, arithmetic and copies ran while one was open for 13% of the time, Pallas kernels for 0%

profile of v1, /device:TPU:8, one launch (start us, length us, event | category | flops | bytes accessed | tf_op | source)
XLA Modules:
  0.0 187.0 jit_solution(13611265761450962420)
XLA Ops:
  6.5 0.0 copy-start
  6.5 0.0 copy-start.5
  6.5 0.0 all-gather.2.cloned.1.call-start
  6.5 14.7 %all_gather.6 = bf16[128,2048]{1,0:T(8,128)(2,1)} all-gather(bf16[128,256]{1,0:T(8,128)(2,1)} %param.20), channel_id=1, replica_groups=mesh['sp'=16,'dp'=8] {'dp'}, dimensions={1}, use_global_device_ids=true | all-gather | bytes 589824 | tf_op jit(solution)/shard_map/all_gather | solution.py:78
  21.3 0.0 all-gather.2.cloned.1.call-update
  21.3 1.1 fusion.12
  22.5 0.5 multiply_cosine_fusion.1
  23.0 1.1 fusion.13
  24.1 0.5 subtract_convert_fusion.3
  24.6 0.4 pad_maximum_fusion.1
  25.1 1.0 broadcast_in_dim.12
  26.0 7.9 %all-to-all-start.1 = ((bf16[128,16,128]{2,0,1:T(8,128)(2,1)}), bf16[128,16,128]{2,0,1:T(8,128)(2,1)S(1)}, u32[]{:S(2)}, u32[]{:S(2)}) async-start(bf16[128,16,128]{2,0,1:T(8,128)(2,1)} %bitcast.10), calls=%async_computation.1 | async-start | bytes 1048576 | tf_op jit(solution)/shard_map/all_to_all | solution.py:115
  33.9 0.0 copy-done
  33.9 0.3 fusion.10
  34.3 0.0 copy-done.5
  34.3 0.3 fusion.11
  34.6 0.0 copy-start.2
  34.7 0.9 subtract_convert_fusion.1
  35.5 1.5 pad_maximum_fusion
  37.0 14.5 %all-to-all-done.1 = bf16[128,16,128]{2,0,1:T(8,128)(2,1)S(1)} async-done(((bf16[128,16,128]{2,0,1:T(8,128)(2,1)}), bf16[128,16,128]{2,0,1:T(8,128)(2,1)S(1)}, u32[]{:S(2)}, u32[]{:S(2)}) %all-to-all-start.1) | async-done | bytes 524320 | tf_op jit(solution)/shard_map/all_to_all | solution.py:115
  51.5 3.6 %all-to-all-start = ((bf16[128,16,128]{2,0,1:T(8,128)(2,1)}), bf16[128,16,128]{2,0,1:T(8,128)(2,1)S(1)}, u32[]{:S(2)}, u32[]{:S(2)}) async-start(bf16[128,16,128]{2,0,1:T(8,128)(2,1)} %pad_maximum_fusion), calls=%async_computation | async-start | bytes 1048576 | tf_op jit(solution)/shard_map/all_to_all | solution.py:114
  55.1 0.0 copy-done.2
  55.1 11.1 %all-to-all-done = bf16[128,16,128]{2,0,1:T(8,128)(2,1)S(1)} async-done(((bf16[128,16,128]{2,0,1:T(8,128)(2,1)}), bf16[128,16,128]{2,0,1:T(8,128)(2,1)S(1)}, u32[]{:S(2)}, u32[]{:S(2)}) %all-to-all-start) | async-done | bytes 524320 | tf_op jit(solution)/shard_map/all_to_all | solution.py:114
  66.2 0.9 broadcast_in_dim.13
  67.1 3.6 %all-to-all-start.2 = ((bf16[128,16,128]{2,0,1:T(8,128)(2,1)}), bf16[128,16,128]{2,0,1:T(8,128)(2,1)S(1)}, u32[]{:S(2)}, u32[]{:S(2)}) async-start(bf16[128,16,128]{2,0,1:T(8,128)(2,1)} %bitcast.15), calls=%async_computation.2 | async-start | bytes 1048576 | tf_op jit(solution)/shard_map/all_to_all | solution.py:118
  70.7 17.7 %all-to-all-done.2 = bf16[128,16,128]{2,0,1:T(8,128)(2,1)S(1)} async-done(((bf16[128,16,128]{2,0,1:T(8,128)(2,1)}), bf16[128,16,128]{2,0,1:T(8,128)(2,1)S(1)}, u32[]{:S(2)}, u32[]{:S(2)}) %all-to-all-start.2) | async-done | bytes 524320 | tf_op jit(solution)/shard_map/all_to_all | solution.py:118
  88.4 0.0 copy-start.4
  88.4 0.0 copy-start.3
  88.4 10.7 %while.10 = (s32[]{:T(128)}, bf16[4,512,128]{2,1,0:T(8,128)(2,1)S(1)}, bf16[4,512,128]{2,1,0:T(8,128)(2,1)S(1)}, bf16[2048,128]{1,0:T(8,128)(2,1)S(1)}, bf16[2048,128]{1,0:T(8,128)(2,1)S(1)}, /*index=5*/s32[]{:T(128)}) while((s32[]{:T(128)}, bf16[4,512,128]{2,1,0:T(8,128)(2,1)S(1)}, bf16[4,512,128]{2,1,0:T(8,128)(2,1)S(1)}, ...), condition=%wide.region_5.6_spmd, body=%wide.region_2.5_spmd.sunk | while | flops 546372608 | bytes 13903949 | solution.py:73
  88.4 0.8 multiply_reduce_fusion.2
  89.2 0.8 fusion.26
  90.0 1.1 fusion.27
  91.1 0.8 multiply_reduce_fusion.2
  91.9 0.8 fusion.26
  92.7 1.1 fusion.27
  93.7 0.8 multiply_reduce_fusion.2
  94.5 0.8 fusion.26
  95.4 1.1 fusion.27
  96.4 0.8 multiply_reduce_fusion.2
  97.2 0.8 fusion.26
  98.0 1.1 fusion.27
  99.1 0.0 copy-start.1
  99.1 0.5 broadcast.198
  99.6 1.0 reduce
  100.6 0.9 reshape.183
  101.6 3.6 %all-to-all-start.3 = ((bf16[16,2,8192]{2,1,0:T(2,128)(2,1)}), bf16[16,2,8192]{2,1,0:T(2,128)(2,1)S(1)}, u32[]{:S(2)}, u32[]{:S(2)}) async-start(bf16[16,2,8192]{2,1,0:T(2,128)(2,1)} %reshape.183), calls=%async_computation.3 | async-start | bytes 1048576 | tf_op jit(solution)/shard_map/all_to_all | solution.py:127
  105.1 0.0 copy-done.4
  105.2 0.7 copy.58
  105.9 0.0 copy-done.3
  105.9 0.7 copy.59.routes_ref
  106.6 8.6 %all-to-all-done.3 = bf16[16,2,8192]{2,1,0:T(2,128)(2,1)S(1)} async-done(((bf16[16,2,8192]{2,1,0:T(2,128)(2,1)}), bf16[16,2,8192]{2,1,0:T(2,128)(2,1)S(1)}, u32[]{:S(2)}, u32[]{:S(2)}) %all-to-all-start.3) | async-done | bytes 524320 | tf_op jit(solution)/shard_map/all_to_all | solution.py:127
  115.2 0.7 reshape.184
  116.0 0.1 copy.60
  116.0 0.3 copy.57
  116.3 0.0 all-gather.2.cloned.1.call-done
  116.3 0.0 copy-done.1
  116.4 5.7 %convolution_add_fusion.mixed_ref = f32[128,2048]{1,0:T(8,128)} fusion(bf16[128,2048]{0,1:T(8,128)(2,1)S(1)} %bitcast.68, bf16[2048,2048]{1,0:T(8,128)(2,1)} %all-gather.2.cloned.1.call-done, bf16[1,128,2048]{2,1,0:T(8,128)(2,1)S(1)} %copy-done.1), kind=kOutput, calls=%fused_computation.13 | convolution fusion | flops 1074266112 | bytes 10485760 | tf_op jit(solution)/shard_map/dot_general | solution.py:83
  122.1 56.2 %experts.1 = bf16[128,2048]{1,0:T(8,128)(2,1)} custom-call(f32[128,2048]{1,0:T(8,128)} %convolution_add_fusion.mixed_ref, f32[1,2048]{1,0:T(1,128)} %bitcast.76, s32[128,2]{1,0:T(8,128)} %copy.59.routes_ref, s32[2,128]{1,0:T(2,128)} %bitcast.77, f32[128,2]{1,0:T(8,128)} %bitcast.74, bf16[2048,1792]{1,0:T(8,128)(2,1)} %bitcast.65, ...), custom_call_target="tpu_custom_call" | custom-call | tf_op jit(solution)/shard_map/experts/pallas_call | solution.py:279
  178.3 1.9 %copy.75 = bf16[1,128,2048]{2,1,0:T(8,128)(2,1)} copy(bf16[1,128,2048]{2,1,0:T(8,128)(2,1)} %bitcast.70) | data formatting | bytes 1048576
  (7 shorter events, 0.1 us)
Async XLA Ops:
  6.5 27.4 %copy-start = (bf16[1,128,16,128]{3,2,1,0:T(8,128)(2,1)S(1)}, bf16[1,128,16,128]{3,2,1,0:T(8,128)(2,1)}, u32[]{:S(2)}) copy-start(bf16[1,128,16,128]{3,2,1,0:T(8,128)(2,1)} %param.15) | copy-start | bytes 1572868
  6.5 27.8 %copy-start.5 = (f32[128]{0:T(128)S(1)}, f32[128]{0:T(128)}, u32[]{:S(2)}) copy-start(f32[128]{0:T(128)} %param.18) | copy-start | bytes 1540
  6.5 109.8 %all-gather.2.cloned.1.call-start = ((), (), s32[]{:S(2)}) async-start(), calls=%async_computation.4 | async-start | bytes 8912896 | tf_op jit(solution)/shard_map/all_gather | solution.py:85
  26.0 25.5 %all-to-all-start.1 = ((bf16[128,16,128]{2,0,1:T(8,128)(2,1)}), bf16[128,16,128]{2,0,1:T(8,128)(2,1)S(1)}, u32[]{:S(2)}, u32[]{:S(2)}) async-start(bf16[128,16,128]{2,0,1:T(8,128)(2,1)} %bitcast.10), calls=%async_computation.1 | async-start | bytes 1048576 | tf_op jit(solution)/shard_map/all_to_all | solution.py:115
  34.6 20.5 %copy-start.2 = (bf16[1,128,4,128]{3,2,1,0:T(4,128)(2,1)S(1)}, bf16[1,128,4,128]{3,2,1,0:T(4,128)(2,1)}, u32[]{:S(2)}) copy-start(bf16[1,128,4,128]{3,2,1,0:T(4,128)(2,1)} %param.17) | copy-start | bytes 393220
  51.5 14.7 %all-to-all-start = ((bf16[128,16,128]{2,0,1:T(8,128)(2,1)}), bf16[128,16,128]{2,0,1:T(8,128)(2,1)S(1)}, u32[]{:S(2)}, u32[]{:S(2)}) async-start(bf16[128,16,128]{2,0,1:T(8,128)(2,1)} %pad_maximum_fusion), calls=%async_computation | async-start | bytes 1048576 | tf_op jit(solution)/shard_map/all_to_all | solution.py:114
  67.1 21.3 %all-to-all-start.2 = ((bf16[128,16,128]{2,0,1:T(8,128)(2,1)}), bf16[128,16,128]{2,0,1:T(8,128)(2,1)S(1)}, u32[]{:S(2)}, u32[]{:S(2)}) async-start(bf16[128,16,128]{2,0,1:T(8,128)(2,1)} %bitcast.15), calls=%async_computation.2 | async-start | bytes 1048576 | tf_op jit(solution)/shard_map/all_to_all | solution.py:118
  88.4 16.8 %copy-start.4 = (f32[1,128,2]{1,2,0:T(2,128)S(1)}, f32[1,128,2]{1,2,0:T(2,128)}, u32[]{:S(2)}) copy-start(f32[1,128,2]{1,2,0:T(2,128)} %param.27) | copy-start | bytes 3076
  88.4 17.5 %copy-start.3 = (s32[1,128,2]{1,2,0:T(2,128)S(1)}, s32[1,128,2]{1,2,0:T(2,128)}, u32[]{:S(2)}) copy-start(s32[1,128,2]{1,2,0:T(2,128)} %param.26) | copy-start | bytes 3076
  99.1 17.3 %copy-start.1 = (bf16[1,128,2048]{2,1,0:T(8,128)(2,1)S(1)}, bf16[1,128,2048]{2,1,0:T(8,128)(2,1)}, u32[]{:S(2)}) copy-start(bf16[1,128,2048]{2,1,0:T(8,128)(2,1)} %param.21) | copy-start | bytes 1572868
  101.6 13.7 %all-to-all-start.3 = ((bf16[16,2,8192]{2,1,0:T(2,128)(2,1)}), bf16[16,2,8192]{2,1,0:T(2,128)(2,1)S(1)}, u32[]{:S(2)}, u32[]{:S(2)}) async-start(bf16[16,2,8192]{2,1,0:T(2,128)(2,1)} %reshape.183), calls=%async_computation.3 | async-start | bytes 1048576 | tf_op jit(solution)/shard_map/all_to_all | solution.py:127
Sparse Core Ops, SparseCore 0:
  21.4 83.7 all-gather.1

commit v2 on v1

--- a/solution.py
+++ b/solution.py
@@ -1,3 +1,5 @@
+import math
+
 import jax
 import jax.numpy as jnp
 from jax import lax
@@ -6,132 +8,255 @@
 from jax.sharding import PartitionSpec as P
 
 MESH = pl.DeviceIdType.MESH
-
-GRID_W = 64
-
-
 EPS = 1e-06
 THETA = 10000.0
 
 
-def rotate_half(vector, position):
-    half_size = vector.shape[-1] // 2
-    inverse = THETA ** (-jnp.arange(half_size, dtype=jnp.float32) / half_size)
-    angles = position[:, None] * inverse[None, :]
-    cosine = jnp.cos(angles)[:, None, :]
-    sine_part = jnp.sin(angles)[:, None, :]
-    first_part = vector[..., :half_size]
-    second_part = vector[..., half_size:]
-    return jnp.concatenate(
-        [
-            first_part * cosine - second_part * sine_part,
-            first_part * sine_part + second_part * cosine,
+PIECES = (
+    ((0, 64), ("z", "x", "y")),
+    ((64, 96), ("y", "x", "z")),
+    ((96, 128), ("y", "z", "x")),
+)
+AXES = ("y", "z", "x")
+
+
+def front_kernel(
+    q_ref, k_ref, v_ref, q_gain_ref, k_gain_ref, residual_hbm, weight_hbm,
+    out_ref,
+    q_f32, q_send, q_all, kv_send, kv_all, o_send, o_all, att_v, w_all, residual_v,
+    local_sem, k1_s, k1_r, k2_s, k2_r, q_s, q_r, o_s, o_r, w_s, w_r, p_s, p_r,
+):
+    me = lax.axis_index("sp")
+    dp = lax.axis_index("dp")
+    at = {"z": me // 4, "x": me % 4, "y": dp // 2}
+    z, x, y, core = at["z"], at["x"], at["y"], dp % 2
+
+    def device(axis, off):
+        if axis == "core":
+            return {"dp": y * 2 + (1 - core)}
+        v = (at[axis] + off + 4) % 4
+        if axis == "y":
+            return {"dp": v * 2 + core}
+        return {"sp": v * 4 + x if axis == "z" else z * 4 + v}
+
+    def remote(src, dst, ssem, rsem, target):
+        return pltpu.make_async_remote_copy(
+            src_ref=src, dst_ref=dst, send_sem=ssem, recv_sem=rsem,
+            device_id=target, device_id_type=MESH,
+        )
+
+    def piece_ref(p, gathered, axis, value, cols=None, owner=None):
+        rows = pl.ds(PIECES[p][0][0], PIECES[p][0][1] - PIECES[p][0][0])
+        index = [core if owner is None else owner]
+        for name in AXES:
+            if name == axis:
+                index.append(value)
+            else:
+                index.append(slice(None) if name in gathered else at[name])
+        index += [rows, slice(None) if cols is None else cols]
+        return w_all.at[tuple(index)]
+
+    load_w = pltpu.make_async_copy(weight_hbm, w_all.at[core, y, z, x], local_sem.at[0])
+    load_r = pltpu.make_async_copy(residual_hbm, residual_v, local_sem.at[1])
+    load_w.start()
+    load_r.start()
+    barrier = pltpu.get_barrier_semaphore()
+    for axis in AXES:
+        for off in (1, 2, 3):
+            pl.semaphore_signal(barrier, inc=1, device_id=device(axis, off), device_id_type=MESH)
+    pl.semaphore_signal(barrier, inc=1, device_id=device("core", 1), device_id_type=MESH)
+
+    lane = lax.broadcasted_iota(jnp.int32, (128, 128), 1)
+    position = lax.broadcasted_iota(jnp.int32, (128, 128), 0) + me * 128
+    place = jnp.where(lane < 64, position >> 6, position & 63).astype(jnp.float32)
+    rate = jnp.exp((lane & 31).astype(jnp.float32) * (-math.log(THETA) / 32))
+    angle = place * rate
+    cosine = jnp.cos(angle)
+    low = (lane & 63) < 32
+    sine = jnp.where(low, -jnp.sin(angle), jnp.sin(angle))
+
+    def turned(rows, gain):
+        scaled = rows * lax.rsqrt(jnp.mean(rows * rows, axis=-1, keepdims=True) + EPS) * gain
+        other = jnp.where(low, pltpu.roll(scaled, 96, 1), pltpu.roll(scaled, 32, 1))
+        return (scaled * cosine + other * sine).astype(jnp.bfloat16)
+
+    for h in range(4):
+        part = slice(h * 128, h * 128 + 128)
+        kv_send[h, 0] = turned(k_ref[:, part].astype(jnp.float32), k_gain_ref[...])
+        kv_send[h, 1] = v_ref[:, part]
+    kv_all[x * 4 + z] = kv_send[z]
+    q_f32[...] = q_ref[...].reshape(2048, 128).astype(jnp.float32)
+    pl.semaphore_wait(barrier, 10)
+
+    def kv_in(off):
+        return remote(kv_send.at[(z + off) % 4], kv_all.at[x * 4 + z], k1_s.at[off], k1_r.at[off], device("z", off))
+
+    started = []
+
+    def start(copy):
+        copy.start()
+        started.append(copy)
+
+    def spread(off):
+        slot = kv_all.at[x * 4 + (z - off + 4) % 4]
+        for dx in (1, 3, 2):
+            start(remote(slot, slot, k2_s.at[off, dx], k2_r.at[off, dx], device("x", dx)))
+
+    for off in (1, 3, 2):
+        start(kv_in(off))
+    spread(0)
+
+    for h in range(16):
+        q_send[h // 4, h % 4] = turned(q_f32[pl.ds(h, 128, stride=16), :], q_gain_ref[...])
+    q_all[z] = q_send[z]
+    for off in (2, 1, 3):
+        start(remote(q_send.at[(z + off) % 4], q_all.at[z], q_s.at[off], q_r.at[off], device("z", off)))
+
+    def phase_copy(p, n, off, outgoing):
+        order = PIECES[p][1]
+        gathered, axis = order[:n], order[n]
+        value = at[axis] if outgoing else (at[axis] - off + 4) % 4
+        block = piece_ref(p, gathered, axis, value)
+        return remote(block, block, w_s.at[p, n, off], w_r.at[p, n, off], device(axis, off))
+
+    def half_copy(p, side, outgoing):
+        order = PIECES[p][1]
+        axis = order[2]
+        step = 1 if side == 0 else 3
+        value = (at[axis] - step + 4) % 4 if outgoing else (at[axis] + 2) % 4
+        block = piece_ref(p, order[:2], axis, value, cols=pl.ds(side * 128, 128))
+        n = 2 if side == 0 else 0
+        return remote(block, block, w_s.at[p, 2, n], w_r.at[p, 2, n], device(axis, step))
+
+    def across(p, part, outgoing):
+        order = PIECES[p][1]
+        axis = order[2]
+        owner = core if outgoing else 1 - core
+        cols = None
+        if part == 0:
+            value = at[axis]
+        elif part < 3:
+            value = (at[axis] - (1, 3)[part - 1] + 4) % 4
+        else:
+            value = (at[axis] + 2) % 4
+            cols = pl.ds((part - 3) * 128, 128)
+        block = piece_ref(p, order[:2], axis, value, cols=cols, owner=owner)
+        return remote(block, block, p_s.at[p, part], p_r.at[p, part], device("core", 1))
+
+    load_w.wait()
+    for p in range(3):
+        for off in (1, 3, 2):
+            start(phase_copy(p, 0, off, True))
+
+    for off in (1, 3, 2):
+        incoming = kv_all.at[x * 4 + (z - off + 4) % 4]
+        remote(incoming, incoming, k1_s.at[off], k1_r.at[off], device("z", off)).wait_recv()
+        spread(off)
+
+    for p in range(3):
+        for off in (1, 3, 2):
+            phase_copy(p, 0, off, False).wait_recv()
+        for off in (1, 3, 2):
+            start(phase_copy(p, 1, off, True))
+
+    for off in range(4):
+        for dx in (1, 3, 2):
+            slot = kv_all.at[((x - dx + 4) % 4) * 4 + (z - off + 4) % 4]
+            remote(slot, slot, k2_s.at[off, dx], k2_r.at[off, dx], device("x", dx)).wait_recv()
+
+    for p in range(3):
+        for off in (1, 3, 2):
+            phase_copy(p, 1, off, False).wait_recv()
+        for off in (1, 3):
+            start(phase_copy(p, 2, off, True))
+        start(across(p, 0, True))
+
+    keys = kv_all[:, 0].reshape(2048, 128)
+    vals = kv_all[:, 1].reshape(2048, 128)
+    factor = 128 ** -0.5 * math.log2(math.e)
+
+    def attend(source, target):
+        for half in range(2):
+            query = q_all[source, pl.ds(half * 2, 2)].reshape(256, 128)
+            scores = lax.dot_general(
+                query, keys, (((1,), (1,)), ((), ())), preferred_element_type=jnp.float32
+            )
+            top = jnp.max(scores, axis=-1, keepdims=True)
+            power = jnp.exp2((scores - top) * factor)
+            share = (power * (1.0 / jnp.sum(power, axis=-1, keepdims=True))).astype(jnp.bfloat16)
+            mixed = jnp.dot(share, vals, preferred_element_type=jnp.float32).astype(jnp.bfloat16)
+            target[pl.ds(half * 2, 2)] = mixed.reshape(2, 128, 128)
+
+    for off in (2, 1, 3):
+        source = (z - off + 4) % 4
+        slot = q_all.at[source]
+        remote(slot, slot, q_s.at[off], q_r.at[off], device("z", off)).wait_recv()
+        attend(source, o_send.at[source])
+        start(remote(o_send.at[source], o_all.at[z], o_s.at[off], o_r.at[off], device("z", -off)))
+    attend(z, o_all.at[z])
+
+    for p in (1, 2, 0):
+        for side, off in ((0, 1), (1, 3)):
+            phase_copy(p, 2, off, False).wait_recv()
+            start(half_copy(p, side, True))
+            start(across(p, 1 + side, True))
+    for p in (1, 2, 0):
+        for side in (0, 1):
+            half_copy(p, side, False).wait_recv()
+            start(across(p, 3 + side, True))
+    for off in (2, 1, 3):
+        slot = o_all.at[(z + off) % 4]
+        remote(slot, slot, o_s.at[off], o_r.at[off], device("z", off)).wait_recv()
+    for h in range(16):
+        att_v[:, h * 128:h * 128 + 128] = o_all[h // 4, h % 4]
+    for p in range(3):
+        for part in range(5):
+            across(p, part, False).wait_recv()
+    load_r.wait()
+    for c in range(2):
+        for b in range(4):
+            first = (b * 2 + c) * 256
+            cols = slice(first, first + 256)
+            summed = jnp.dot(
+                att_v[...], w_all[c, b].reshape(2048, 256), preferred_element_type=jnp.float32
+            )
+            out_ref[:, cols] = residual_v[:, cols].astype(jnp.float32) + summed
+    for copy in started:
+        copy.wait_send()
+
+
+def front(queries, key_rows, values, query_gain, key_gain, residual, out_weight):
+    vmem = pl.BlockSpec(memory_space=pltpu.VMEM)
+    hbm = pl.BlockSpec(memory_space=pl.ANY)
+    dma = pltpu.SemaphoreType.DMA
+    heads = pltpu.VMEM((4, 4, 128, 128), jnp.bfloat16)
+    return pl.pallas_call(
+        front_kernel,
+        out_shape=jax.ShapeDtypeStruct((128, 2048), jnp.float32),
+        in_specs=[vmem] * 5 + [hbm] * 2,
+        out_specs=vmem,
+        scratch_shapes=[
+            pltpu.VMEM((2048, 128), jnp.float32),
+            heads, heads,
+            pltpu.VMEM((4, 2, 128, 128), jnp.bfloat16),
+            pltpu.VMEM((16, 2, 128, 128), jnp.bfloat16),
+            heads, heads,
+            pltpu.VMEM((128, 2048), jnp.bfloat16),
+            pltpu.VMEM((2, 4, 4, 4, 128, 256), jnp.bfloat16),
+            pltpu.VMEM((128, 2048), jnp.bfloat16),
+            dma((2,)),
+            dma((4,)), dma((4,)), dma((4, 4)), dma((4, 4)),
+            dma((4,)), dma((4,)), dma((4,)), dma((4,)),
+            dma((3, 3, 4)), dma((3, 3, 4)), dma((3, 5)), dma((3, 5)),
         ],
-        axis=-1,
+        compiler_params=pltpu.CompilerParams(
+            collective_id=0, has_side_effects=True, vmem_limit_bytes=48 << 20
+        ),
+        name="front",
+    )(
+        queries, key_rows.reshape(128, 512), values.reshape(128, 512),
+        query_gain.reshape(1, 128), key_gain.reshape(1, 128), residual, out_weight,
     )
-
-
-def normalize_rotate(vector, gain, positions):
-    as_float = vector.astype(jnp.float32)
-    scaled = (
-        as_float * lax.rsqrt(jnp.mean(as_float * as_float, axis=-1, keepdims=True) + EPS) * gain
-    )
-    grid_row = (positions // GRID_W).astype(jnp.float32)
-    column = (positions % GRID_W).astype(jnp.float32)
-    quarter = scaled.shape[-1] // 2
-    turned = jnp.concatenate(
-        [rotate_half(scaled[..., :quarter], grid_row), rotate_half(scaled[..., quarter:], column)],
-        axis=-1,
-    )
-    return turned.astype(jnp.bfloat16)
-
-
-def softmax_rows(scores):
-    row_max = jnp.max(scores, axis=-1, keepdims=True)
-    exponent = jnp.exp(scores - row_max)
-    return (exponent / jnp.sum(exponent, axis=-1, keepdims=True)).astype(jnp.bfloat16)
-
-
-def attend_block(query_rows, key_rows, value_rows):
-    scores = jnp.einsum(
-        "qd,kd->qk", query_rows, key_rows, preferred_element_type=jnp.float32
-    ) * query_rows.shape[-1] ** (-0.5)
-    weights = softmax_rows(scores)
-    return jnp.dot(weights, value_rows, preferred_element_type=jnp.float32).astype(jnp.bfloat16)
-
-
-def attend_heads(head_query, head_key, head_value):
-    length, head_count, head_width = head_query.shape
-    block_size = min(512, length)
-    key_slice = head_key[:, 0]
-    value_slice = head_value[:, 0]
-    query_blocks = head_query[:, 0].reshape(length // block_size, block_size, head_width)
-
-    def one_block(query_block):
-        return attend_block(query_block, key_slice, value_slice)
-
-    outputs = [lax.map(one_block, query_blocks).reshape(length, head_width)]
-    return jnp.stack(outputs, axis=1)
-
-
-def gather_columns(out_weight):
-    return lax.all_gather(out_weight, "dp", axis=1, tiled=True)
-
-
-def project_tokens(attended, out_weight):
-    out_cols = gather_columns(out_weight)
-    return jnp.dot(
-        attended,
-        lax.all_gather(out_cols, "sp", axis=0, tiled=True),
-        preferred_element_type=jnp.float32,
-    )
-
-
-def on_device(
-    queries,
-    key_rows,
-    values,
-    query_gain,
-    key_gain,
-    out_weight,
-    residual,
-    norm_gain,
-    expert_gate,
-    expert_up,
-    expert_down,
-    routes,
-    route_weight,
-):
-    tok_count = queries.shape[1]
-    head_count = queries.shape[2]
-    head_width = queries.shape[3]
-    group_size = head_count // key_rows.shape[2]
-    positions = lax.axis_index("sp") * tok_count + jnp.arange(tok_count, dtype=jnp.int32)
-    rot_query = normalize_rotate(queries[0], query_gain, positions)
-    rot_key = normalize_rotate(key_rows[0], key_gain, positions)
-    value_rows = values[0]
-    head_query, head_key, head_value = (
-        lax.all_to_all(rot_query, "sp", split_axis=1, concat_axis=0, tiled=True),
-        lax.all_to_all(
-            jnp.repeat(rot_key, group_size, axis=1), "sp", split_axis=1, concat_axis=0, tiled=True
-        ),
-        lax.all_to_all(
-            jnp.repeat(value_rows, group_size, axis=1),
-            "sp",
-            split_axis=1,
-            concat_axis=0,
-            tiled=True,
-        ),
-    )
-    by_heads = attend_heads(head_query, head_key, head_value)
-    returned_heads = lax.all_to_all(by_heads, "sp", split_axis=0, concat_axis=1, tiled=True)
-    projected = project_tokens(
-        returned_heads.reshape(tok_count, head_count * head_width), out_weight
-    )
-    mixed_sum = residual[0].astype(jnp.float32) + projected
-    return moe(
-        mixed_sum, norm_gain, routes[0], route_weight[0], expert_gate[0], expert_up[0], expert_down[0]
-    )[None]
 
 
 def offset_of(i):
@@ -300,6 +425,29 @@
     )(mixed_sum, norm_gain.reshape(1, -1), routes, routes.T, route_weight, gate, up, down)
 
 
+def on_device(
+    queries,
+    key_rows,
+    values,
+    query_gain,
+    key_gain,
+    out_weight,
+    residual,
+    norm_gain,
+    expert_gate,
+    expert_up,
+    expert_down,
+    routes,
+    route_weight,
+):
+    mixed_sum = front(
+        queries[0], key_rows[0], values[0], query_gain, key_gain, residual[0], out_weight
+    )
+    return moe(
+        mixed_sum, norm_gain, routes[0], route_weight[0], expert_gate[0], expert_up[0], expert_down[0]
+    )[None]
+
+
 def solution(mesh):
     in_specs = (
         P("dp", "sp", None, None),

time: 188 us -> 130 us (0.69)
  the two profiles are of different devices: /device:TPU:8 before, /device:TPU:15 now
where the time goes in v2:
time: 130 us
  Pallas kernels  119 us (92%)
  local copies, waits for them, and re-layouts  10.9 us (8%)
    pallas_call x1, Pallas kernels, moe(): pl.pallas_call(moe_kernel, out_shape=jax.ShapeDtypeStruct((128, 2048), jn...  69.8 us
    pallas_call x1, Pallas kernels, front(): pl.pallas_call(front_kernel, out_shape=jax.ShapeDtypeStruct((128, 2048),...  49.2 us
    unnamed x14, local copies, waits for them, and re-layouts  8.47 us

profile of v2, /device:TPU:15, one launch (start us, length us, event | category | flops | bytes accessed | tf_op | source)
XLA Modules:
  0.0 129.9 jit_solution(18427097132862017974)
XLA Ops:
  0.0 1.4 %copy.14 = f32[1,128,2]{2,1,0:T(8,128)} copy(f32[1,128,2]{1,2,0:T(2,128)} %param.25) | data formatting | bytes 2048 | tf_op args[12]
  1.4 1.4 %copy.15.routes_ref = s32[128,2]{1,0:T(8,128)} copy(s32[128,2]{0,1:T(2,128)} %bitcast.33) | data formatting | bytes 2048 | tf_op jit(solution)/shard_map/squeeze | solution.py:447
  2.8 1.0 copy_bitcast_fusion
  3.8 0.0 copy-start.1
  3.8 1.0 copy-done.1
  4.9 0.0 copy-start.2
  4.9 1.0 copy-done.2
  5.9 0.0 copy-start.3
  5.9 0.8 copy-done.3
  6.7 0.0 copy-start.4
  6.7 0.7 copy-done.4
  7.4 0.0 copy-start.5
  7.4 0.7 copy-done.5
  8.1 49.2 %front.1.mixed_ref = f32[128,2048]{1,0:T(8,128)S(1)} custom-call(bf16[128,16,128]{2,1,0:T(8,128)(2,1)S(1)} %bitcast.21, bf16[128,512]{1,0:T(8,128)(2,1)S(1)} %get-tuple-element.6.k_ref, bf16[128,512]{1,0:T(8,128)(2,1)S(1)} %get-tuple-element.5.v_ref, f32[1,128]{1,0:T(1,128)S(1)} %bitcast.23, f32[1,128]{1,0:T(1,128)S(1)} %bitcast.24, ...), custom_call_target="tpu_custom_call" | custom-call | tf_op jit(solution)/shard_map/front/pallas_call | solution.py:233
  57.2 0.0 copy-start
  57.2 1.0 copy-done
  58.2 69.8 %experts.1 = bf16[128,2048]{1,0:T(8,128)(2,1)} custom-call(f32[128,2048]{1,0:T(8,128)} %copy-done, f32[1,2048]{1,0:T(1,128)} %bitcast.32, s32[128,2]{1,0:T(8,128)} %copy.15.routes_ref, s32[2,128]{1,0:T(2,128)} %bitcast.34, f32[128,2]{1,0:T(8,128)} %bitcast.29, bf16[2048,1792]{1,0:T(8,128)(2,1)} %bitcast.25, bf16[2048,1792]{1,0:T(8,128)(2,1)} %bitcast.26, ...), custom_call_target="tpu_custom_call" | custom-call | tf_op jit(solution)/shard_map/experts/pallas_call | solution.py:404
  128.1 1.9 %copy.21 = bf16[1,128,2048]{2,1,0:T(8,128)(2,1)} copy(bf16[1,128,2048]{2,1,0:T(8,128)(2,1)} %bitcast.28) | data formatting | bytes 1048576
Async XLA Ops:
  3.8 1.0 copy-start.1
  4.9 1.0 copy-start.2
  5.9 0.8 copy-start.3
  6.7 0.7 copy-start.4
  7.4 0.7 copy-start.5
  57.2 1.0 copy-start

commit v3 on v2

v3 whole, which is shorter than its diff:
```python
import math

import jax
import jax.numpy as jnp
from jax import lax
from jax.experimental import pallas as pl
from jax.experimental.pallas import tpu as pltpu
from jax.sharding import PartitionSpec as P

MESH = pl.DeviceIdType.MESH
EPS = 1e-06
THETA = 10000.0
PIECES = (
    ((0, 64), ("z", "x", "y")),
    ((64, 96), ("y", "x", "z")),
    ((96, 128), ("y", "z", "x")),
)
AXES = ("y", "z", "x")


def offset_of(i):
    q = i // 4
    return (q % 2) * 2 + q // 2, i % 4


def peer_of(z, x, dz, dx):
    return ((z + dz) % 4) * 4 + (x + dx) % 4


def experts_of_slots(slots, z, x):
    i = slots >> 5
    q = i >> 2
    dz = ((q & 1) << 1) | (q >> 1)
    return (((z + dz) & 3) << 2) | ((x + (i & 3)) & 3)


def to_bf16(mask):
    return jnp.where(mask, 1.0, 0.0).astype(jnp.bfloat16)


def layer_kernel(
    q_hbm, k_hbm, v_hbm, q_gain_hbm, k_gain_hbm, weight_hbm, residual_hbm, norm_gain_hbm,
    gate_hbm, up_hbm, down_hbm, routes_hbm, share_hbm,
    out_hbm,
    q_raw, k_raw, v_raw, q_gain_ref, k_gain_ref, norm_gain_ref, routes_ref, share_ref,
    k_f32, v_f32, q_f32, q_send, q_all, kv_send, kv_all, o_send, o_all, att_v, w_all, residual_v,
    mixed_ref, pick_v, take_v,
    gate_v, up_v, down_v, send_v, recv_v, res_v, ret_v, hid_v, out_v,
    local_sem, k1_s, k1_r, k2_s, k2_r, q_s, q_r, o_s, o_r, w_s, w_r, p_s, p_r,
    ds_sem, dr_sem, rs_sem, rr_sem,
):
    me = lax.axis_index("sp")
    dp = lax.axis_index("dp")
    at = {"z": me // 4, "x": me % 4, "y": dp // 2}
    z, x, y, core = at["z"], at["x"], at["y"], dp % 2

    def device(axis, off):
        if axis == "core":
            return {"dp": y * 2 + (1 - core)}
        v = (at[axis] + off + 4) % 4
        if axis == "y":
            return {"dp": v * 2 + core}
        return {"sp": v * 4 + x if axis == "z" else z * 4 + v}

    def remote(src, dst, ssem, rsem, target):
        return pltpu.make_async_remote_copy(
            src_ref=src, dst_ref=dst, send_sem=ssem, recv_sem=rsem,
            device_id=target, device_id_type=MESH,
        )

    def piece_ref(p, gathered, axis, value, cols=None, owner=None):
        rows = pl.ds(PIECES[p][0][0], PIECES[p][0][1] - PIECES[p][0][0])
        index = [core if owner is None else owner]
        for name in AXES:
            if name == axis:
                index.append(value)
            else:
                index.append(slice(None) if name in gathered else at[name])
        index += [rows, slice(None) if cols is None else cols]
        return w_all.at[tuple(index)]

    barrier = pltpu.get_barrier_semaphore()
    for i in range(1, 16):
        pl.semaphore_signal(
            barrier, inc=1, device_id={"sp": peer_of(z, x, *offset_of(i))}, device_id_type=MESH
        )
    for off in (1, 2, 3):
        pl.semaphore_signal(barrier, inc=1, device_id=device("y", off), device_id_type=MESH)
    pl.semaphore_signal(barrier, inc=1, device_id=device("core", 1), device_id_type=MESH)
    loads = [
        pltpu.make_async_copy(src, dst, local_sem.at[n])
        for n, (src, dst) in enumerate(
            (
                (k_hbm, k_raw), (v_hbm, v_raw), (k_gain_hbm, k_gain_ref), (q_gain_hbm, q_gain_ref),
                (q_hbm, q_raw), (weight_hbm, w_all.at[core, y, z, x]), (residual_hbm, residual_v),
                (norm_gain_hbm, norm_gain_ref), (routes_hbm, routes_ref), (share_hbm, share_ref),
                (gate_hbm, gate_v), (up_hbm, up_v), (down_hbm, down_v),
            )
        )
    ]
    for load in loads:
        load.start()

    lane = lax.broadcasted_iota(jnp.int32, (128, 128), 1)
    position = lax.broadcasted_iota(jnp.int32, (128, 128), 0) + me * 128
    place = jnp.where(lane < 64, position >> 6, position & 63).astype(jnp.float32)
    rate = jnp.exp((lane & 31).astype(jnp.float32) * (-math.log(THETA) / 32))
    angle = place * rate
    cosine = jnp.cos(angle)
    low = (lane & 63) < 32
    sine = jnp.where(low, -jnp.sin(angle), jnp.sin(angle))

    def turned(rows, gain):
        scaled = rows * lax.rsqrt(jnp.mean(rows * rows, axis=-1, keepdims=True) + EPS) * gain
        other = jnp.where(low, pltpu.roll(scaled, 96, 1), pltpu.roll(scaled, 32, 1))
        return (scaled * cosine + other * sine).astype(jnp.bfloat16)

    for load in loads[:4]:
        load.wait()
    k_f32[...] = k_raw[...].astype(jnp.float32)
    v_f32[...] = v_raw[...].astype(jnp.float32)
    for h in range(4):
        kv_send[h, 0] = turned(k_f32[:, h, :], k_gain_ref[...])
        kv_send[h, 1] = v_f32[:, h, :].astype(jnp.bfloat16)
    kv_all[x * 4 + z] = kv_send[z]
    loads[4].wait()
    q_f32[...] = q_raw[...].reshape(2048, 128).astype(jnp.float32)
    pl.semaphore_wait(barrier, 19)

    def kv_in(off):
        return remote(kv_send.at[(z + off) % 4], kv_all.at[x * 4 + z], k1_s.at[off], k1_r.at[off], device("z", off))

    started = []

    def start(copy):
        copy.start()
        started.append(copy)

    def spread(off):
        slot = kv_all.at[x * 4 + (z - off + 4) % 4]
        for dx in (1, 3, 2):
            start(remote(slot, slot, k2_s.at[off, dx], k2_r.at[off, dx], device("x", dx)))

    for off in (1, 3, 2):
        start(kv_in(off))
    spread(0)

    for h in range(16):
        q_send[h // 4, h % 4] = turned(q_f32[pl.ds(h, 128, stride=16), :], q_gain_ref[...])
    q_all[z] = q_send[z]
    for off in (2, 1, 3):
        start(remote(q_send.at[(z + off) % 4], q_all.at[z], q_s.at[off], q_r.at[off], device("z", off)))

    def phase_copy(p, n, off, outgoing):
        order = PIECES[p][1]
        gathered, axis = order[:n], order[n]
        value = at[axis] if outgoing else (at[axis] - off + 4) % 4
        block = piece_ref(p, gathered, axis, value)
        return remote(block, block, w_s.at[p, n, off], w_r.at[p, n, off], device(axis, off))

    def half_copy(p, side, outgoing):
        order = PIECES[p][1]
        axis = order[2]
        step = 1 if side == 0 else 3
        value = (at[axis] - step + 4) % 4 if outgoing else (at[axis] + 2) % 4
        block = piece_ref(p, order[:2], axis, value, cols=pl.ds(side * 128, 128))
        n = 2 if side == 0 else 0
        return remote(block, block, w_s.at[p, 2, n], w_r.at[p, 2, n], device(axis, step))

    def across(p, part, outgoing):
        order = PIECES[p][1]
        axis = order[2]
        owner = core if outgoing else 1 - core
        cols = None
        if part == 0:
            value = at[axis]
        elif part < 3:
            value = (at[axis] - (1, 3)[part - 1] + 4) % 4
        else:
            value = (at[axis] + 2) % 4
            cols = pl.ds((part - 3) * 128, 128)
        block = piece_ref(p, order[:2], axis, value, cols=cols, owner=owner)
        return remote(block, block, p_s.at[p, part], p_r.at[p, part], device("core", 1))

    loads[5].wait()
    for p in range(3):
        for off in (1, 3, 2):
            start(phase_copy(p, 0, off, True))

    for off in (1, 3, 2):
        incoming = kv_all.at[x * 4 + (z - off + 4) % 4]
        remote(incoming, incoming, k1_s.at[off], k1_r.at[off], device("z", off)).wait_recv()
        spread(off)

    for p in range(3):
        for off in (1, 3, 2):
            phase_copy(p, 0, off, False).wait_recv()
        for off in (1, 3, 2):
            start(phase_copy(p, 1, off, True))

    for load in loads[7:10]:
        load.wait()
    slots = lax.broadcasted_iota(jnp.int32, (512, 128), 0)
    rows = lax.broadcasted_iota(jnp.int32, (512, 128), 1)
    expert = experts_of_slots(slots, z, x)
    named = (routes_ref[0:1, :] == expert) | (routes_ref[1:2, :] == expert)
    before_r = lax.broadcasted_iota(jnp.int32, (128, 128), 0)
    before_c = lax.broadcasted_iota(jnp.int32, (128, 128), 1)
    same = (before_r >> 6) == (before_c >> 6)
    upper = to_bf16((before_r < before_c) & same)
    lower = to_bf16((before_c < before_r) & same)
    rank = jnp.dot(to_bf16(named), upper, preferred_element_type=jnp.float32)
    wanted = ((slots & 31) - ((rows >> 6) << 4)).astype(jnp.float32)
    pick_v[...] = to_bf16(named & (rank == wanted))
    slots_t = lax.broadcasted_iota(jnp.int32, (128, 512), 1)
    rows_t = lax.broadcasted_iota(jnp.int32, (128, 512), 0)
    expert_t = experts_of_slots(slots_t, z, x).astype(jnp.float32)

    def column(row):
        return jnp.sum(jnp.where(before_r == before_c, row, 0.0), axis=-1, keepdims=True)

    first = column(routes_ref[0:1, :].astype(jnp.float32)) == expert_t
    second = column(routes_ref[1:2, :].astype(jnp.float32)) == expert_t
    rank_t = jnp.dot(lower, to_bf16(first | second), preferred_element_type=jnp.float32)
    here = rank_t == ((slots_t & 31) - ((rows_t >> 6) << 4)).astype(jnp.float32)
    take_v[0] = to_bf16(first & here)
    take_v[1] = to_bf16(second & here)

    for off in range(4):
        for dx in (1, 3, 2):
            slot = kv_all.at[((x - dx + 4) % 4) * 4 + (z - off + 4) % 4]
            remote(slot, slot, k2_s.at[off, dx], k2_r.at[off, dx], device("x", dx)).wait_recv()

    for p in range(3):
        for off in (1, 3, 2):
            phase_copy(p, 1, off, False).wait_recv()
        for off in (1, 3):
            start(phase_copy(p, 2, off, True))
        start(across(p, 0, True))

    keys = kv_all[:, 0].reshape(2048, 128)
    vals = kv_all[:, 1].reshape(2048, 128)
    factor = 128 ** -0.5 * math.log2(math.e)

    def attend(source, target):
        for half in range(2):
            query = q_all[source, pl.ds(half * 2, 2)].reshape(256, 128)
            scores = lax.dot_general(
                query, keys, (((1,), (1,)), ((), ())), preferred_element_type=jnp.float32
            )
            top = jnp.max(scores, axis=-1, keepdims=True)
            power = jnp.exp2((scores - top) * factor)
            share = (power * (1.0 / jnp.sum(power, axis=-1, keepdims=True))).astype(jnp.bfloat16)
            mixed = jnp.dot(share, vals, preferred_element_type=jnp.float32).astype(jnp.bfloat16)
            target[pl.ds(half * 2, 2)] = mixed.reshape(2, 128, 128)

    for off in (2, 1, 3):
        source = (z - off + 4) % 4
        slot = q_all.at[source]
        remote(slot, slot, q_s.at[off], q_r.at[off], device("z", off)).wait_recv()
        attend(source, o_send.at[source])
        start(remote(o_send.at[source], o_all.at[z], o_s.at[off], o_r.at[off], device("z", -off)))
    attend(z, o_all.at[z])

    for p in (1, 2, 0):
        for side, off in ((0, 1), (1, 3)):
            phase_copy(p, 2, off, False).wait_recv()
            start(half_copy(p, side, True))
            start(across(p, 1 + side, True))
    for p in (1, 2, 0):
        for side in (0, 1):
            half_copy(p, side, False).wait_recv()
            start(across(p, 3 + side, True))
    for off in (2, 1, 3):
        slot = o_all.at[(z + off) % 4]
        remote(slot, slot, o_s.at[off], o_r.at[off], device("z", off)).wait_recv()
    for h in range(16):
        att_v[:, h * 128:h * 128 + 128] = o_all[h // 4, h % 4]
    for p in range(3):
        for part in range(5):
            across(p, part, False).wait_recv()
    loads[6].wait()
    for c in range(2):
        for b in range(4):
            first = (b * 2 + c) * 256
            cols = slice(first, first + 256)
            summed = jnp.dot(
                att_v[...], w_all[c, b].reshape(2048, 256), preferred_element_type=jnp.float32
            )
            mixed_ref[:, cols] = residual_v[:, cols].astype(jnp.float32) + summed

    mixed = mixed_ref[...]
    scale = lax.rsqrt(jnp.mean(mixed * mixed, axis=-1, keepdims=True) + EPS)
    normed = (mixed * scale * norm_gain_ref[...]).astype(jnp.bfloat16)

    def exchange(i, src, dst, ssem, rsem, dz, dx):
        return pltpu.make_async_remote_copy(
            src_ref=src.at[pl.ds(i * 32, 32)],
            dst_ref=dst.at[pl.ds(i * 32, 32)],
            send_sem=ssem.at[i],
            recv_sem=rsem.at[i],
            device_id={"sp": peer_of(z, x, dz, dx)},
            device_id_type=MESH,
        )

    outgoing = []
    for i in range(1, 16):
        dz, dx = offset_of(i)
        outgoing.append(exchange(i, send_v, recv_v, ds_sem, dr_sem, dz, dx))
    for c in range(2):
        part = slice(c * 256, c * 256 + 256)
        for n in range(4):
            cols = slice(n * 512, n * 512 + 512)
            sent = jnp.dot(
                pick_v[part], normed[:, cols], preferred_element_type=jnp.float32
            ).astype(jnp.bfloat16)
            send_v[part, cols] = sent
            if c == 0:
                recv_v[0:32, cols] = sent[0:32]
        for i in range(max(1, c * 8), c * 8 + 8):
            outgoing[i - 1].start()


    returning = []
    for i in range(1, 16):
        dz, dx = offset_of(i)
        returning.append(exchange(i, res_v, ret_v, rs_sem, rr_sem, -dz, -dx))
    loads[10].wait()
    loads[11].wait()
    for c in range(2):
        for i in range(max(1, c * 8), c * 8 + 8):
            outgoing[i - 1].wait_recv()
        part = slice(c * 256, c * 256 + 256)
        for n in range(7):
            cols = slice(n * 256, n * 256 + 256)
            gate = jnp.dot(recv_v[part], gate_v[:, cols], preferred_element_type=jnp.float32)
            up = jnp.dot(recv_v[part], up_v[:, cols], preferred_element_type=jnp.float32)
            hid_v[:, cols] = (gate / (1.0 + jnp.exp(-gate)) * up).astype(jnp.bfloat16)
        if c == 0:
            loads[12].wait()
        for n in range(8):
            cols = slice(n * 256, n * 256 + 256)
            done = jnp.dot(
                hid_v[...], down_v[:, cols], preferred_element_type=jnp.float32
            ).astype(jnp.bfloat16)
            res_v[part, cols] = done
            if c == 0:
                ret_v[0:32, cols] = done[0:32]
        for i in range(max(1, c * 8), c * 8 + 8):
            returning[i - 1].start()
    for back in returning:
        back.wait_recv()
    shares = [column(share_ref[k:k + 1, :]) for k in range(2)]
    writes = []
    for n in range(4):
        cols = slice(n * 512, n * 512 + 512)
        got = ret_v[:, cols]
        one = jnp.dot(take_v[0], got, preferred_element_type=jnp.float32)
        two = jnp.dot(take_v[1], got, preferred_element_type=jnp.float32)
        total = mixed_ref[:, cols] + (one * shares[0] + two * shares[1])
        out_v[:, cols] = total.astype(jnp.bfloat16)
        writes.append(pltpu.make_async_copy(out_v.at[:, cols], out_hbm.at[:, cols], local_sem.at[13 + n]))
        writes[-1].start()
    for copy in started + outgoing + returning:
        copy.wait_send()
    for write in writes:
        write.wait()


def layer(
    queries, key_rows, values, query_gain, key_gain, out_weight, residual, norm_gain,
    gate, up, down, routes, route_weight,
):
    dma = pltpu.SemaphoreType.DMA

    def bf16(*shape):
        return pltpu.VMEM(shape, jnp.bfloat16)

    def f32(*shape):
        return pltpu.VMEM(shape, jnp.float32)

    heads = bf16(4, 4, 128, 128)
    rows = bf16(512, 2048)
    return pl.pallas_call(
        layer_kernel,
        out_shape=jax.ShapeDtypeStruct((128, 2048), jnp.bfloat16),
        in_specs=[pl.BlockSpec(memory_space=pl.ANY)] * 13,
        out_specs=pl.BlockSpec(memory_space=pl.ANY),
        scratch_shapes=[
            bf16(128, 16, 128), bf16(128, 4, 128), bf16(128, 4, 128), f32(1, 128), f32(1, 128),
            f32(1, 2048), pltpu.VMEM((2, 128), jnp.int32), f32(2, 128),
            f32(128, 4, 128), f32(128, 4, 128), f32(2048, 128), heads, heads,
            bf16(4, 2, 128, 128), bf16(16, 2, 128, 128), heads, heads,
            bf16(128, 2048), bf16(2, 4, 4, 4, 128, 256), bf16(128, 2048),
            f32(128, 2048), bf16(512, 128), bf16(2, 128, 512),
            bf16(2048, 1792), bf16(2048, 1792), bf16(1792, 2048),
            rows, rows, rows, rows, bf16(256, 1792), bf16(128, 2048),
            dma((17,)),
            dma((4,)), dma((4,)), dma((4, 4)), dma((4, 4)),
            dma((4,)), dma((4,)), dma((4,)), dma((4,)),
            dma((3, 3, 4)), dma((3, 3, 4)), dma((3, 5)), dma((3, 5)),
            dma((16,)), dma((16,)), dma((16,)), dma((16,)),
        ],
        compiler_params=pltpu.CompilerParams(
            collective_id=0, has_side_effects=True, vmem_limit_bytes=63 << 20
        ),
        name="layer",
    )(
        queries, key_rows, values, query_gain.reshape(1, -1), key_gain.reshape(1, -1), out_weight,
        residual, norm_gain.reshape(1, -1), gate, up, down, routes.T, route_weight.T,
    )


def on_device(
    queries,
    key_rows,
    values,
    query_gain,
    key_gain,
    out_weight,
    residual,
    norm_gain,
    expert_gate,
    expert_up,
    expert_down,
    routes,
    route_weight,
):
    return layer(
        queries[0], key_rows[0], values[0], query_gain, key_gain, out_weight, residual[0], norm_gain,
        expert_gate[0], expert_up[0], expert_down[0], routes[0], route_weight[0],
    )[None]


def solution(mesh):
    in_specs = (
        P("dp", "sp", None, None),
        P("dp", "sp", None, None),
        P("dp", "sp", None, None),
        P(),
        P(),
        P("sp", "dp"),
        P("dp", "sp", None),
        P(),
        P("sp", None, None),
        P("sp", None, None),
        P("sp", None, None),
        P("dp", "sp", None),
        P("dp", "sp", None),
    )
    out_specs = P("dp", "sp", None)
    return jax.shard_map(
        on_device, mesh=mesh, in_specs=in_specs, out_specs=out_specs, check_vma=False
    )
```

time: 130 us -> 114 us (0.88)
  the two profiles are of different devices: /device:TPU:15 before, /device:TPU:7 now
where the time goes in v3:
time: 114 us; the launch traced here: 112 us
  Pallas kernels  111 us (97%)
  local copies, waits for them, and re-layouts  1.88 us (2%)
    pallas_call x1, Pallas kernels, layer(): pl.pallas_call(layer_kernel, out_shape=jax.ShapeDtypeStruct((128, 2048),...  111 us

profile of v3, /device:TPU:7, one launch (start us, length us, event | category | flops | bytes accessed | tf_op | source)
XLA Modules:
  0.0 112.5 jit_solution(131470442428094335)
XLA Ops:
  0.0 110.6 %layer.1 = bf16[128,2048]{1,0:T(8,128)(2,1)} custom-call(bf16[128,16,128]{2,1,0:T(8,128)(2,1)} %bitcast.21, bf16[128,4,128]{2,1,0:T(4,128)(2,1)} %bitcast.23, bf16[128,4,128]{2,1,0:T(4,128)(2,1)} %bitcast.24, f32[1,128]{1,0:T(1,128)} %bitcast.28, f32[1,128]{1,0:T(1,128)} %bitcast.29, bf16[128,256]{1,0:T(8,128)(2,1)} %weight_hbm.1, ...), custom_call_target="tpu_custom_call" | custom-call | tf_op jit(solution)/shard_map/layer/pallas_call | solution.py:384
  110.6 1.9 %copy.15 = bf16[1,128,2048]{2,1,0:T(8,128)(2,1)} copy(bf16[1,128,2048]{2,1,0:T(8,128)(2,1)} %bitcast.20) | data formatting | bytes 1048576
